TPU v7x, 32 devices: a whole 2x2x4 slice. The times are simulated.
32 devices in a mesh: sp: 8 (over z, y), tp: 4 (over x, core).
Axes of the slice: x: 2, y: 2, z: 4, core: 2. Of those that a mesh axis runs over, the one named last changes fastest.
Arguments:
- tokens: bfloat16 [2, 4096, 2048], P(None, ('sp', 'tp')), may hold values from -6.5 to 6.5, as said below
- norm_gain: float32 [2048], replicated, may hold values from 0.1 to 1.9
- w_gate: bfloat16 [2048, 4096], P('sp', 'tp'), may hold values from -0.125 to 0.125
- w_value: bfloat16 [2048, 4096], P('sp', 'tp'), may hold values from -0.125 to 0.125
- w_write: bfloat16 [2048, 512], P('sp', 'tp'), may hold values from -0.125 to 0.125
- w_read: bfloat16 [2048, 512], P('sp', 'tp'), may hold values from -0.125 to 0.125
- w_step: bfloat16 [2048, 64], replicated, may hold values from -0.125 to 0.125
- conv_value: float32 [4, 4096], replicated, may hold values from -3 to 3
- conv_write: float32 [4, 512], replicated, may hold values from -3 to 3
- conv_read: float32 [4, 512], replicated, may hold values from -3 to 3
- step_bias: float32 [64], replicated, as said below
- decay_log: float32 [64], replicated, may hold values from 0 to 0.7
- skip_gain: float32 [64], replicated, may hold values from 0.1 to 1.9
- out_gain: float32 [4096], replicated, may hold values from 0.1 to 1.9
- w_out: bfloat16 [4096, 2048], P(None, 'sp'), may hold values from -0.09375 to 0.09375
Outputs:
- mixed: bfloat16 [2, 4096, 2048], P(None, ('sp', 'tp'))
Inputs may be any that keep to these rules, and one draw needn't show every extreme that they name: `tokens`: activations of order one whose mean along a direction drifts slowly over each sequence. `step_bias`: even heads take step offsets between -5.8 and -5.0, odd heads offsets near log(0.12 to 0.33) - log(4096).
All inputs are finite; a program needn't handle non-finite values.
Results may differ from a plain program's by a relative error of at most 0.005.
The roundings to bfloat16 on the way count: a program that leaves them out, or rounds other values in their place, can miss the bound.
Values may be sent and summed in bfloat16 or wider, within the bound.
A program may use at most 192 MiB of HBM per device.

v0:
```python
import jax
import jax.numpy as jnp
from jax import lax
from jax.sharding import PartitionSpec as P

BLOCK = 64


EPSILON = 1e-06
HIGHEST = lax.Precision.HIGHEST


def shifted(x, axis, by):
    devices = lax.axis_size(axis)
    pairs = [(i, i + by) for i in range(devices) if 0 <= i + by < devices]
    return lax.ppermute(x, axis, pairs)


def entering(part, axis, combine, identity):
    place = lax.axis_index(axis)
    gathered = jax.tree.map(lambda a: lax.all_gather(a, axis), part)
    state = jax.tree.map(lambda a, e: jnp.zeros_like(a) + jnp.asarray(e, a.dtype), part, identity)

    def one(step, state):
        return combine(
            state, jax.tree.map(lambda a: lax.dynamic_index_in_dim(a, step, 0, False), gathered)
        )

    return lax.fori_loop(0, place, one, state)


def rms_scale(values, gain_vec):
    return (
        values * lax.rsqrt(jnp.mean(values * values, axis=-1, keepdims=True) + EPSILON) * gain_vec
    )


def convolve(local_rows, earlier, kernel):
    tap_count = kernel.shape[0]
    length = local_rows.shape[1]
    padded = jnp.concatenate([earlier, local_rows], axis=1).astype(jnp.float32)
    running = padded[:, 0:length, :] * kernel[0]
    for offset in range(1, tap_count):
        running = running + padded[:, offset : offset + length, :] * kernel[offset]
    return jax.nn.silu(running)


def merge_states(earlier, later):
    return (earlier[0] * later[0], earlier[1] * later[0][:, :, None, None] + later[1])


def body(
    tokens,
    norm_gain,
    w_gate,
    w_value,
    w_write,
    w_read,
    w_step,
    conv_value,
    conv_write,
    conv_read,
    step_bias,
    decay_log,
    skip_gain,
    out_gain,
    w_out,
):
    seq_count, own_rows, model_width = tokens.shape
    group_devs = lax.axis_size("tp")
    tp_rank = lax.axis_index("tp")
    head_count = w_step.shape[1]
    local_heads = head_count // group_devs
    channels = w_gate.shape[1]
    head_dim = channels // local_heads
    state_dim = w_write.shape[1]
    tap_count = conv_value.shape[0]
    group_rows = own_rows * group_devs
    normed = rms_scale(tokens.astype(jnp.float32), norm_gain).astype(jnp.bfloat16)
    whole_gate, whole_value, whole_write, whole_read, whole_out = (
        lax.all_gather(w_gate, "sp", axis=0, tiled=True),
        lax.all_gather(w_value, "sp", axis=0, tiled=True),
        lax.all_gather(w_write, "sp", axis=0, tiled=True),
        lax.all_gather(w_read, "sp", axis=0, tiled=True),
        lax.all_gather(w_out, "sp", axis=1, tiled=True),
    )
    first_head = tp_rank * local_heads
    step_cols = lax.dynamic_slice_in_dim(w_step, first_head, local_heads, 1)
    projections = (whole_gate, whole_value, whole_write, whole_read)

    def empty_rows(cols, dtype):
        return jnp.zeros((seq_count, group_rows, cols), dtype)

    initial = (
        empty_rows(channels, jnp.bfloat16),
        empty_rows(channels, jnp.bfloat16),
        empty_rows(state_dim, jnp.bfloat16),
        empty_rows(state_dim, jnp.bfloat16),
        empty_rows(local_heads, jnp.float32),
    )
    shard_piece = lax.all_gather(normed, "tp", axis=1, tiled=True)
    piece_rows = shard_piece.shape[1]
    flat_piece = shard_piece.reshape(seq_count * piece_rows, model_width)
    updated = []
    for target, weight in zip(initial[:4], projections):
        projected = jnp.dot(flat_piece, weight, preferred_element_type=jnp.float32)
        projected = projected.astype(jnp.bfloat16).reshape(seq_count, piece_rows, weight.shape[1])
        updated.append(projected)
    step_piece = jnp.dot(flat_piece, step_cols, preferred_element_type=jnp.float32)
    step_piece = step_piece.reshape(seq_count, piece_rows, local_heads)
    updated.append(step_piece)
    gate_in, value_in, write_in, read_in, step_raw = tuple(updated)
    keep_from = group_rows - tap_count + 1
    tail_rows = jnp.concatenate(
        [value_in[:, keep_from:], write_in[:, keep_from:], read_in[:, keep_from:]], axis=2
    )
    before = shifted(tail_rows, "sp", 1)
    kernel_value = lax.dynamic_slice_in_dim(conv_value, first_head * head_dim, channels, 1)
    kernel_write = lax.dynamic_slice_in_dim(conv_write, tp_rank * state_dim, state_dim, 1)
    kernel_read = lax.dynamic_slice_in_dim(conv_read, tp_rank * state_dim, state_dim, 1)
    value_conv = convolve(value_in, before[:, :, :channels], kernel_value)
    write_conv = convolve(write_in, before[:, :, channels : channels + state_dim], kernel_write)
    read_conv = convolve(read_in, before[:, :, channels + state_dim :], kernel_read)
    step_size = jax.nn.softplus(
        step_raw + lax.dynamic_slice_in_dim(step_bias, first_head, local_heads, 0)
    )
    decay_rate = -jnp.exp(lax.dynamic_slice_in_dim(decay_log, first_head, local_heads, 0))
    skip_local = lax.dynamic_slice_in_dim(skip_gain, first_head, local_heads, 0)
    block_count = group_rows // BLOCK
    value_blocks = value_conv.reshape(seq_count, block_count, BLOCK, local_heads, head_dim)
    step_blocks = jnp.moveaxis(step_size.reshape(seq_count, block_count, BLOCK, local_heads), 3, 2)
    write_blocks = write_conv.reshape(seq_count, block_count, BLOCK, state_dim)
    read_blocks = read_conv.reshape(seq_count, block_count, BLOCK, state_dim)
    log_decay = jnp.cumsum(step_blocks * decay_rate[:, None], axis=3)
    value_steps = value_blocks * jnp.moveaxis(step_blocks, 3, 2)[..., None]
    causal_mask = jnp.arange(BLOCK)[:, None] >= jnp.arange(BLOCK)[None, :]
    log_gap = log_decay[..., :, None] - log_decay[..., None, :]
    weights = jnp.exp(jnp.where(causal_mask, log_gap, -jnp.inf))
    intersect = jnp.einsum("skln,skmn->sklm", read_blocks, write_blocks, precision=HIGHEST)
    scores = weights * intersect[:, :, None]
    inner = jnp.einsum("skhlm,skmhp->sklhp", scores, value_steps, precision=HIGHEST)
    block_decay = log_decay[..., -1]
    fade_out = jnp.exp(block_decay[..., None] - log_decay)
    states = jnp.einsum(
        "skmn,skhm,skmhp->skhpn", write_blocks, fade_out, value_steps, precision=HIGHEST
    )
    run_sum = jnp.cumsum(block_decay, axis=1)
    run_before = run_sum - block_decay
    block_ids = jnp.arange(block_count)
    later_mask = (block_ids[:, None] > block_ids[None, :])[:, :, None]
    between = jnp.exp(
        jnp.where(later_mask, run_before[:, :, None, :] - run_sum[:, None, :, :], -jnp.inf)
    )
    prev_state = jnp.einsum("skjh,sjhpn->skhpn", between, states, precision=HIGHEST)
    total_fade = jnp.exp(run_sum[:, -1:, :] - run_sum)
    dev_state = jnp.einsum("sjh,sjhpn->shpn", total_fade, states, precision=HIGHEST)
    dev_decay = jnp.exp(run_sum[:, -1, :])
    identity = (jnp.ones_like(dev_decay), jnp.zeros_like(dev_state))
    incoming = entering((dev_decay, dev_state), "sp", merge_states, identity)[1]
    read_scale = jnp.exp(log_decay)
    local_part = jnp.einsum(
        "skln,skhpn,skhl->sklhp", read_blocks, prev_state, read_scale, precision=HIGHEST
    )
    outer_part = jnp.einsum(
        "skln,shpn,skhl->sklhp",
        read_blocks,
        incoming,
        jnp.exp(run_before[..., None] + log_decay),
        precision=HIGHEST,
    )
    carried = local_part + outer_part
    heads_out = (inner + carried + skip_local[:, None] * value_blocks).reshape(
        seq_count, group_rows, channels
    )
    gated = (heads_out * jax.nn.silu(gate_in.astype(jnp.float32))).astype(jnp.bfloat16)
    token_rows = lax.all_to_all(gated, "tp", split_axis=1, concat_axis=2, tiled=True)
    mixed_in = rms_scale(token_rows.astype(jnp.float32), out_gain).astype(jnp.bfloat16)
    flat_mixed = mixed_in.reshape(seq_count * own_rows, mixed_in.shape[2])
    result = jnp.dot(flat_mixed, whole_out, preferred_element_type=jnp.float32).astype(jnp.bfloat16)
    return result.reshape(seq_count, own_rows, model_width)


def solution(mesh):
    in_specs = (
        P(None, ("sp", "tp"), None),
        P(),
        P("sp", "tp"),
        P("sp", "tp"),
        P("sp", "tp"),
        P("sp", "tp"),
        P(),
        P(),
        P(),
        P(),
        P(),
        P(),
        P(),
        P(),
        P(None, "sp"),
    )
    out_specs = P(None, ("sp", "tp"), None)
    return jax.shard_map(body, mesh=mesh, in_specs=in_specs, out_specs=out_specs, check_vma=False)
```

profile of v0, /device:TPU:0, one launch (start us, length us, event | category | flops | bytes accessed | tf_op | source)
XLA Modules:
  0.0 570.5 jit_solution(64083504945850999)
XLA Ops:
  6.6 1.6 fusion.33
  8.2 2.5 fusion.35
  10.8 0.7 all-gather.10.cloned.1.call-update
  11.5 0.7 all-gather.12.cloned.1.call-update
  12.4 33.1 %all_gather.30 = bf16[2048,128]{1,0:T(8,128)(2,1)S(1)} all-gather(bf16[256,128]{1,0:T(8,128)(2,1)S(1)} %copy-done.10), channel_id=1, replica_groups=mesh['sp'=8,'tp'=4] {'sp'}, dimensions={0}, use_global_device_ids=true | all-gather | bytes 589824 | tf_op jit(solution)/shard_map/all_gather | solution.py:83
  45.5 32.9 %all_gather.31 = bf16[2048,128]{1,0:T(8,128)(2,1)S(1)} all-gather(bf16[256,128]{1,0:T(8,128)(2,1)S(1)} %copy-done.11), channel_id=1, replica_groups=mesh['sp'=8,'tp'=4] {'sp'}, dimensions={0}, use_global_device_ids=true | all-gather | bytes 589824 | tf_op jit(solution)/shard_map/all_gather | solution.py:84
  78.4 1.3 constant_dynamic-slice_fusion.1
  79.7 0.6 slice_bitcast_fusion.3
  80.3 1.6 constant_dynamic-slice_fusion
  81.9 3.4 compare_select_fusion
  85.4 3.5 reduce_window_sum.24
  89.4 3.6 convolution_convert_fusion.4
  93.0 1.2 convolution_convert_fusion.3
  95.1 0.8 exponential_bitcast_fusion.2
  96.0 28.8 %all-gather.10.cloned.1.call-done = bf16[2048,1024]{1,0:T(8,128)(2,1)} async-done(((bf16[256,1024]{1,0:T(8,128)(2,1)}), bf16[2048,1024]{1,0:T(8,128)(2,1)}) %all-gather.10.cloned.1.call-update) | async-done | bytes 4194320 | tf_op jit(solution)/shard_map/all_gather | solution.py:82
  124.8 7.9 %convolution_convert_fusion.2 = bf16[1024,1024]{1,0:T(8,128)(2,1)S(1)} fusion(bf16[1024,2048]{1,0:T(8,128)(2,1)} %bitcast.120, bf16[2048,1024]{1,0:T(8,128)(2,1)} %all-gather.10.cloned.1.call-done), kind=kOutput, calls=%fused_computation.53 | convolution fusion | flops 4296015872 | bytes 10485760 | tf_op jit(solution)/shard_map/dot_general | solution.py:106
  132.7 0.6 pad_maximum_fusion
  133.4 3.1 collective-permute-start
  136.4 0.6 fusion.63
  137.2 1.1 copy.101
  138.3 0.8 copy.119
  139.1 0.7 slice.132
  139.9 0.6 maximum_convert_fusion
  140.5 4.6 divide_multiply_fusion
  145.1 7.4 %reshape.114 = f32[2,8,64,16,64]{4,3,2,1,0:T(8,128)} reshape(f32[2,512,1024]{2,1,0:T(8,128)} %divide_multiply_fusion) | data formatting | bytes 8388608 | tf_op jit(solution)/shard_map/reshape | solution.py:130
  152.5 0.7 fusion.62
  153.7 9.0 %broadcast_multiply_fusion = (f32[2,8,64,16,64]{4,3,2,1,0:T(8,128)S(1)}, f32[2,8,64,16,64]{4,3,2,1,0:T(8,128)}) fusion(f32[2,8,64,16]{3,2,1,0:T(8,128)S(1)} %copy.101, f32[2,8,64,16,64]{4,3,2,1,0:T(8,128)} %reshape.114, f32[2,8,64,16]{3,2,1,0:T(8,128)S(1)} %copy.98), kind=kLoop, calls=%fused_computation.33 | loop fusion | flops 2097152 | bytes 12713984 | tf_op jit(solution)/shard_map/skmn,skhm,skmhp->skhpn/dot_general | solution.py:144
  162.7 15.2 %fusion.3 = f32[2,8,16,64,128]{4,3,2,1,0:T(8,128)S(1)} fusion(f32[2,8,64,128,1]{3,2,4,1,0:T(8,128)S(1)} %bitcast.117, f32[2,8,64,16,64]{4,3,2,1,0:T(8,128)S(1)} %get-tuple-element.60), kind=kOutput, calls=%fused_computation.6 | convolution fusion | flops 1610612736 | bytes 13107200 | tf_op jit(solution)/shard_map/skmn,skhm,skmhp->skhpn/dot_general | solution.py:144
  177.9 11.7 %fusion.11 = f32[2,16,1,64,128]{4,2,3,1,0:T(1,128)} fusion(f32[2,8,16,1,1]{1,3,4,2,0:T(1,128)S(1)} %copy.119, f32[2,8,16,64,128]{4,3,2,1,0:T(8,128)S(1)} %fusion.3), kind=kOutput, calls=%fused_computation.14 | convolution fusion | flops 25165824 | bytes 9438208 | tf_op jit(solution)/shard_map/sjh,sjhpn->shpn/dot_general | solution.py:156
  190.5 18.6 %all-gather = f32[16,1,16]{2,1,0:T(1,128)S(1)} all-gather(f32[2,1,16]{2,1,0:T(1,128)S(1)} %copy-done.13), channel_id=2, replica_groups=mesh['sp'=8,'tp'=4] {'sp'}, dimensions={0}, use_global_device_ids=true | all-gather | bytes 1152 | tf_op jit(solution)/shard_map/all_gather | solution.py:21
  209.1 9.4 %convolution_convert_fusion.1 = bf16[1024,1024]{1,0:T(8,128)(2,1)} fusion(bf16[1024,2048]{1,0:T(8,128)(2,1)} %bitcast.121, bf16[2048,1024]{1,0:T(8,128)(2,1)} %all-gather.12.cloned.1.call-done), kind=kOutput, calls=%fused_computation.52 | convolution fusion | flops 4296015872 | bytes 10485760 | tf_op jit(solution)/shard_map/dot_general | solution.py:106
  218.4 9.2 %copy.110 = f32[2,8,64,16,64]{2,4,3,1,0:T(8,128)} copy(f32[2,8,64,16,64]{4,3,2,1,0:T(8,128)} %reshape.114) | data formatting | bytes 8388608 | tf_op jit(solution)/shard_map/reshape | solution.py:130
  228.0 0.9 fusion.65
  228.9 17.3 %fusion.30 = f32[2,8,16,64,128]{4,1,3,2,0:T(8,128)} fusion(f32[2,8,16,64,128]{4,3,2,1,0:T(8,128)} %copy-done.2, f32[2,8,16]{1,2,0:T(8,128)S(1)} %copy.104, f32[2,8,16]{1,2,0:T(8,128)S(1)} %copy.103, pred[8,8]{1,0:T(8,128)(4,1)S(1)} %iota_compare_fusion.1), kind=kOutput, calls=%fused_computation.42 | convolution fusion | flops 201330688 | bytes 16779328 | tf_op jit(solution)/shard_map/skjh,sjhpn->skhpn/dot_general | solution.py:154
  246.2 17.5 %fusion.5 = f32[2,8,16,64,64]{4,3,2,1,0:T(8,128)} fusion(f32[2,8,64,16,64]{4,3,2,1,0:T(8,128)S(1)} %bitcast.111, f32[2,8,64,64]{3,2,1,0:T(8,128)S(1)} %fusion.65, f32[2,8,16,64]{3,2,1,0:T(8,128)S(1)} %reduce_window_sum.24, pred[64,64]{1,0:T(8,128)(4,1)S(1)} %iota_compare_fusion), kind=kOutput, calls=%fused_computation.8 | convolution fusion | flops 808452096 | bytes 8720384 | tf_op jit(solution)/shard_map/skhlm,skmhp->sklhp/dot_general | solution.py:141
  263.8 60.0 %all-gather.16.cloned.1.call-done = f32[16,16,64,128]{3,2,1,0:T(8,128)} async-done(((f32[2,16,64,128]{3,2,1,0:T(8,128)}), f32[16,16,64,128]{3,2,1,0:T(8,128)}) %all-gather.16.cloned.1.call-update) | async-done | bytes 8388624 | tf_op jit(solution)/shard_map/all_gather | solution.py:21
  323.9 9.5 %fusion.38 = f32[2,8,64,16,64]{2,4,3,1,0:T(8,128)} fusion(f32[2,8,64,128,1]{3,2,4,1,0:T(8,128)S(1)} %bitcast.115, f32[2,16,64,128]{3,2,1,0:T(8,128)S(1)} %get-tuple-element.49), kind=kOutput, calls=%fused_computation.57 | convolution fusion | flops 1610612736 | bytes 5767168 | tf_op jit(solution)/shard_map/skln,shpn,skhl->sklhp/dot_general | solution.py:164
  333.4 19.5 %fusion = f32[2,8,64,16,64]{2,4,3,1,0:T(8,128)} fusion(f32[2,8,16,64,64]{4,3,2,1,0:T(8,128)} %fusion.5, f32[2,8,64,16,64]{2,4,3,1,0:T(8,128)} %copy.110, f32[2,8,64,16,64]{2,4,3,1,0:T(8,128)} %fusion.38, f32[16]{0:T(128)S(1)} %dynamic_slice.37, f32[2,8,64,16]{2,3,1,0:T(8,128)S(1)} %copy-done.5, f32[2,8,64,16]{2,3,1,0:T(8,128)S(1)} %get-tuple-element.62, ...), kind=kOutput, calls=%fused_computation.3 | convolution fusion | flops 1616904192 | bytes 25821248 | tf_op jit(solution)/shard_map/skln,skhpn,skhl->sklhp/dot_general | solution.py:161
  352.9 9.2 %copy.111 = f32[2,8,64,16,64]{4,3,2,1,0:T(8,128)} copy(f32[2,8,64,16,64]{2,4,3,1,0:T(8,128)} %fusion) | data formatting | bytes 8388608 | tf_op jit(solution)/shard_map/add | solution.py:172
  362.1 8.0 %reshape.117 = f32[2,512,1024]{2,1,0:T(8,128)} reshape(f32[2,8,64,16,64]{4,3,2,1,0:T(8,128)} %copy.111) | data formatting | bytes 8388608 | tf_op jit(solution)/shard_map/reshape | solution.py:172
  370.1 3.5 fusion.26
  373.6 2.2 copy.112
  375.8 28.3 %all_to_all.4 = bf16[2,512,1024]{2,0,1:T(2,128)(2,1)S(1)} all-to-all(bf16[2,512,1024]{2,0,1:T(2,128)(2,1)S(1)} %copy.112), channel_id=1, replica_groups=mesh['sp'=8,'tp'=4] {'tp'}, dimensions={1} | all-to-all | bytes 4194304 | tf_op jit(solution)/shard_map/all_to_all | solution.py:176
  404.1 1.6 copy.113
  405.7 5.8 %copy.123 = f32[32,8,4,1024]{3,1,2,0:T(8,128)} copy(f32[32,8,4,1024]{3,2,1,0:T(4,128)S(1)} %bitcast.113) | data formatting | bytes 8388608
  411.5 2.2 multiply_reduce_fusion
  413.9 137.3 %all-gather.14.cloned.1.call-done = bf16[4096,2048]{1,0:T(8,128)(2,1)} async-done(((bf16[4096,256]{1,0:T(8,128)(2,1)}), bf16[4096,2048]{1,0:T(8,128)(2,1)}) %all-gather.14.cloned.1.call-update) | async-done | bytes 16777232 | tf_op jit(solution)/shard_map/all_gather | solution.py:85
  551.2 12.6 %convolution_convert_fusion = bf16[256,2048]{1,0:T(8,128)(2,1)} fusion(bf16[4096,2048]{1,0:T(8,128)(2,1)} %all-gather.14.cloned.1.call-done, f32[256,4096]{1,0:T(8,128)} %bitcast.124, f32[4096]{0:T(1024)S(1)} %copy-done.18, f32[256]{0:T(256)S(1)} %bitcast.141), kind=kOutput, calls=%fused_computation.45 | convolution fusion | flops 4298637312 | bytes 22037504 | tf_op jit(solution)/shard_map/dot_general | solution.py:179
  (88 shorter events, 3.8 us)
Async XLA Ops:
  6.5 75.3 %copy-start = (bf16[2048,64]{0,1:T(8,128)(2,1)S(1)}, bf16[2048,64]{0,1:T(8,128)(2,1)}, u32[]{:S(2)}) copy-start(bf16[2048,64]{0,1:T(8,128)(2,1)} %param.23) | copy-start | bytes 786436
  6.5 5.7 %copy-start.19 = (f32[64]{0:T(128)S(1)}, f32[64]{0:T(128)}, u32[]{:S(2)}) copy-start(f32[64]{0:T(128)} %param.27) | copy-start | bytes 772
  6.5 5.8 %copy-start.20 = (f32[64]{0:T(128)S(1)}, f32[64]{0:T(128)}, u32[]{:S(2)}) copy-start(f32[64]{0:T(128)} %param.28) | copy-start | bytes 772
  6.5 5.9 %copy-start.10 = (bf16[256,128]{1,0:T(8,128)(2,1)S(1)}, bf16[256,128]{1,0:T(8,128)(2,1)}, u32[]{:S(2)}) copy-start(bf16[256,128]{1,0:T(8,128)(2,1)} %param.21) | copy-start | bytes 196612
  6.5 39.0 %copy-start.11 = (bf16[256,128]{1,0:T(8,128)(2,1)S(1)}, bf16[256,128]{1,0:T(8,128)(2,1)}, u32[]{:S(2)}) copy-start(bf16[256,128]{1,0:T(8,128)(2,1)} %param.22) | copy-start | bytes 196612
  6.5 75.3 %all-gather.8.cloned.1.call-start = ((), (), s32[]{:S(2)}) async-start(), calls=%async_computation.1 | async-start | bytes 5242880 | tf_op jit(solution)/shard_map/all_gather | solution.py:101
  10.7 114.0 %all-gather.10.cloned.1.call-start = ((), (), s32[]{:S(2)}) async-start(), calls=%async_computation.2 | async-start | bytes 4718592 | tf_op jit(solution)/shard_map/all_gather | solution.py:82
  11.5 197.6 %all-gather.12.cloned.1.call-start = ((), (), s32[]{:S(2)}) async-start(), calls=%async_computation.3 | async-start | bytes 4718592 | tf_op jit(solution)/shard_map/all_gather | solution.py:81
  12.2 311.5 %all-gather.16.cloned.1.call-start = ((), (), s32[]{:S(2)}) async-start(), calls=%async_computation.5 | async-start | bytes 9437184 | tf_op jit(solution)/shard_map/all_gather | solution.py:21
  89.4 3.6 copy-start.3
  93.0 1.5 copy-start.6
  94.3 1.7 copy-start.8
  133.4 5.8 %collective-permute-start = (bf16[2,3,1280]{2,1,0:T(4,128)(2,1)}, bf16[2,3,1280]{2,1,0:T(4,128)(2,1)}, u32[]{:S(2)}, u32[]{:S(2)}) collective-permute-start(bf16[2,3,1280]{2,1,0:T(4,128)(2,1)} %pad_maximum_fusion), channel_id=1, source_target_pairs={{0,4},{4,8},{8,12},{12,16},{16,20},{20,24},{24,28},{1,5},{5,9},{9,... | collective-permute-start | bytes 46088 | tf_op jit(solution)/shard_map/ppermute | solution.py:16
  145.1 8.1 %copy-start.7 = (bf16[1024,128]{1,0:T(8,128)(2,1)S(1)}, bf16[1024,128]{1,0:T(8,128)(2,1)}, u32[]{:S(2)}) copy-start(bf16[1024,128]{1,0:T(8,128)(2,1)} %copy-done.6) | copy-start | bytes 786436
  145.1 8.1 %copy-start.9 = (bf16[1024,128]{1,0:T(8,128)(2,1)S(1)}, bf16[1024,128]{1,0:T(8,128)(2,1)}, u32[]{:S(2)}) copy-start(bf16[1024,128]{1,0:T(8,128)(2,1)} %copy-done.8) | copy-start | bytes 786436
  145.1 8.2 %copy-start.14 = (f32[128]{0:T(128)S(1)}, f32[128]{0:T(128)}, u32[]{:S(2)}) copy-start(f32[128]{0:T(128)} %get-tuple-element.75) | copy-start | bytes 1540
  145.1 8.2 %copy-start.15 = (f32[128]{0:T(128)S(1)}, f32[128]{0:T(128)}, u32[]{:S(2)}) copy-start(f32[128]{0:T(128)} %get-tuple-element.76) | copy-start | bytes 1540
  145.1 8.2 %copy-start.16 = (f32[128]{0:T(128)S(1)}, f32[128]{0:T(128)}, u32[]{:S(2)}) copy-start(f32[128]{0:T(128)} %get-tuple-element.77) | copy-start | bytes 1540
  145.1 8.2 %copy-start.17 = (f32[128]{0:T(128)S(1)}, f32[128]{0:T(128)}, u32[]{:S(2)}) copy-start(f32[128]{0:T(128)} %get-tuple-element.78) | copy-start | bytes 1540
  177.8 11.7 %copy-start.2 = (f32[2,8,16,64,128]{4,3,2,1,0:T(8,128)}, f32[2,8,16,64,128]{4,3,2,1,0:T(8,128)S(1)}, u32[]{:S(2)}) copy-start(f32[2,8,16,64,128]{4,3,2,1,0:T(8,128)S(1)} %fusion.3) | copy-start | bytes 25165828
  177.9 12.3 %copy-start.21 = (f32[64]{0:T(128)S(1)}, f32[64]{0:T(128)}, u32[]{:S(2)}) copy-start(f32[64]{0:T(128)} %param.29) | copy-start | bytes 772
  177.9 12.4 %copy-start.12 = (f32[4,128]{1,0:T(4,128)S(1)}, f32[4,128]{1,0:T(4,128)}, u32[]{:S(2)}) copy-start(f32[4,128]{1,0:T(4,128)} %get-tuple-element.86) | copy-start | bytes 6148
  177.9 12.6 %copy-start.13 = (f32[2,1,16]{2,1,0:T(1,128)S(1)}, f32[2,1,16]{2,1,0:T(1,128)}, u32[]{:S(2)}) copy-start(f32[2,1,16]{2,1,0:T(1,128)} %get-tuple-element.74) | copy-start | bytes 388
  189.6 361.6 %all-gather.14.cloned.1.call-start = ((), (), s32[]{:S(2)}) async-start(), calls=%async_computation.4 | async-start | bytes 18874368 | tf_op jit(solution)/shard_map/all_gather | solution.py:85
  227.9 18.3 %slice-start = ((s8[8388608]{0:T(1024)(128)(4,1)}), s8[4194304]{0:T(1024)(128)(4,1)S(1)}, s32[]{:S(2)}) async-start(s8[8388608]{0:T(1024)(128)(4,1)} %bitcast.110), calls=%async_computation.6 | async-start | bytes 8388608
  228.9 17.3 %slice-start.1 = ((s8[8388608]{0:T(1024)(128)(4,1)}), s8[4194304]{0:T(1024)(128)(4,1)S(1)}, s32[]{:S(2)}) async-start(s8[8388608]{0:T(1024)(128)(4,1)} %bitcast.110), calls=%async_computation.7 | async-start | bytes 8388608
  323.9 9.5 %copy-start.5 = (f32[2,8,64,16]{2,3,1,0:T(8,128)S(1)}, f32[2,8,64,16]{2,3,1,0:T(8,128)}, u32[]{:S(2)}) copy-start(f32[2,8,64,16]{2,3,1,0:T(8,128)} %get-tuple-element.64) | copy-start | bytes 196612
  362.1 8.0 %copy-start.4 = (bf16[1024,1024]{1,0:T(8,128)(2,1)S(1)}, bf16[1024,1024]{1,0:T(8,128)(2,1)}, u32[]{:S(2)}) copy-start(bf16[1024,1024]{1,0:T(8,128)(2,1)} %convolution_convert_fusion.1) | copy-start | bytes 6291460
  405.7 145.4 %copy-start.18 = (f32[4096]{0:T(1024)S(1)}, f32[4096]{0:T(1024)}, u32[]{:S(2)}) copy-start(f32[4096]{0:T(1024)} %param.30) | copy-start | bytes 49156
  551.2 12.6 %copy-start.1 = (bf16[2048,64]{0,1:T(8,128)(2,1)S(1)}, bf16[2048,64]{0,1:T(8,128)(2,1)}, u32[]{:S(2)}) copy-start(bf16[2048,64]{0,1:T(8,128)(2,1)} %param.23) | copy-start | bytes 786436
Sparse Core Ops, SparseCore 0:
  10.8 37.1 all-gather.7
  50.2 74.5 all-gather.9
  126.9 71.7 all-gather.11
  200.7 123.0 all-gather.15
  325.6 225.4 all-gather.13
where the time goes:
time: 580 us; the launch traced here: 570 us
  waiting for transfers between devices  228 us (39%)
  matrix products  130 us (22%)
  blocking collectives  113 us (19%)
  local copies, waits for them, and re-layouts  51.9 us (9%)
  other arithmetic  30.8 us (5%)
  between operations  13.8 us (2%)
    all_gather x1, waiting for transfers between devices, body(): lax.all_gather(w_out, 'sp', axis=1, tiled=True)  137 us
    all_gather x1, waiting for transfers between devices, entering(): gathered = jax.tree.map(lambda a: lax.all_gather(a, axis), part)  60 us
    all_gather x1, blocking collectives, body(): lax.all_gather(w_write, 'sp', axis=0, tiled=True)  33.1 us
    all_gather x1, blocking collectives, body(): lax.all_gather(w_read, 'sp', axis=0, tiled=True)  32.9 us
    all_gather x1, waiting for transfers between devices, body(): lax.all_gather(w_value, 'sp', axis=0, tiled=True)  28.8 us
    all_to_all x1, blocking collectives, body(): lax.all_to_all(gated, 'tp', split_axis=1, concat_axis=2, tiled=True)  28.3 us
    dot_general x4, matrix products, body(): projected = jnp.dot(flat_piece, weight, preferred_element_type=jnp.float32)  22.1 us
    dot_general x1, matrix products, body(): jnp.einsum('skln,skhpn,skhl->sklhp', read_blocks, prev_state, read_scale,...  19.5 us
  transfers between devices with their start and end apart: 6, of which 3 were waited for; matrix products, arithmetic and copies ran while one was open for 34% of the time, Pallas kernels for 0%

commit v1 on v0

v1 whole, which is shorter than its diff:
```python
import jax
import jax.numpy as jnp
from jax import lax
from jax.experimental import pallas as pl
from jax.experimental.pallas import tpu as pltpu
from jax.sharding import PartitionSpec as P

EPSILON = 1e-06
HIGHEST = lax.Precision.HIGHEST
HALO = 16
LANES = 128


def shifted(x, axis, by):
    devices = lax.axis_size(axis)
    pairs = [(i, i + by) for i in range(devices) if i + by < devices]
    return lax.ppermute(x, axis, pairs)


def swapped(x, axis, bit):
    devices = lax.axis_size(axis)
    return lax.ppermute(x, axis, [(i, i ^ bit) for i in range(devices)])


def bits_of(axis):
    devices = lax.axis_size(axis)
    bits = []
    bit = devices // 2
    while bit >= 1:
        bits.append(bit)
        bit //= 2
    return bits


def is_power(n):
    return n & (n - 1) == 0


def gather_tokens(x, axis):
    seqs, rows, width = x.shape
    devices = lax.axis_size(axis)
    if not is_power(devices):
        return lax.all_gather(x, axis, axis=1, tiled=True)
    rank = lax.axis_index(axis)
    held = x.reshape(seqs, 1, rows, width)
    for bit in bits_of(axis):
        other = swapped(held, axis, bit)
        upper = (rank & bit) != 0
        first = jnp.where(upper, other, held)
        second = jnp.where(upper, held, other)
        count = held.shape[1]
        held = jnp.stack([first, second], axis=2).reshape(seqs, 2 * count, rows, width)
    return held.reshape(seqs, devices * rows, width)


def total_over(x, axis):
    devices = lax.axis_size(axis)
    if not is_power(devices):
        return jnp.sum(lax.all_gather(x, axis), axis=0)
    for bit in bits_of(axis):
        x = x + swapped(x, axis, bit)
    return x


def incoming_state(state, decay, axis):
    devices = lax.axis_size(axis)
    whole, whole_decay = state, decay
    before, before_decay = None, None
    step = 1
    while step < devices:
        got = shifted(whole.astype(jnp.bfloat16), axis, step).astype(jnp.float32)
        got_decay = shifted(whole_decay, axis, step)
        if before is None:
            before, before_decay = got, got_decay
        else:
            before = got * before_decay + before
            before_decay = got_decay * before_decay
        whole = got * whole_decay + whole
        whole_decay = got_decay * whole_decay
        step *= 2
    if before is None:
        return jnp.zeros_like(state)
    return before


def silu(v):
    return v / (1.0 + jnp.exp(-v))


def dot32(a, b):
    return jnp.dot(a, b, preferred_element_type=jnp.float32)


def mixer_kernel(head_dim, taps_ref, skip_ref, ext_ref, ld_ref, ldt_ref, step_ref, heads_ref, read_ref, state_ref):
    rows = heads_ref.shape[1]
    channels = heads_ref.shape[2]
    state_dim = read_ref.shape[2]
    tap_count = taps_ref.shape[0]
    per = LANES // head_dim
    at = pl.program_id(1)
    start = pl.multiple_of(at * rows, rows)

    @pl.when(at == 0)
    def _():
        state_ref[...] = jnp.zeros_like(state_ref)

    def conv(first, width):
        ext = ext_ref[0, pl.ds(start, rows + HALO), first : first + width].astype(jnp.float32)
        base = HALO - tap_count + 1
        running = None
        for k in range(tap_count):
            term = ext[base + k : base + k + rows] * taps_ref[k : k + 1, first : first + width]
            running = term if running is None else running + term
        return silu(running)

    write = conv(channels, state_dim)
    read = conv(channels + state_dim, state_dim).astype(jnp.bfloat16)
    read_ref[0] = read
    write_t = write.T.astype(jnp.bfloat16)
    cross = dot32(read, write_t)
    line = lax.broadcasted_iota(jnp.int32, (rows, rows), 0)
    column = lax.broadcasted_iota(jnp.int32, (rows, rows), 1)
    causal = line >= column
    log_decay = ld_ref[0]
    log_decay_t = ldt_ref[0]
    steps = step_ref[0]
    lane = lax.broadcasted_iota(jnp.int32, (rows, LANES), 1) // head_dim

    def spread(values, first):
        out = jnp.broadcast_to(values[:, first : first + 1], (values.shape[0], LANES))
        for i in range(1, per):
            part = jnp.broadcast_to(values[:, first + i : first + i + 1], (values.shape[0], LANES))
            out = jnp.where(lane[: values.shape[0]] == i, part, out)
        return out

    for j in range(channels // LANES):
        cols = slice(j * LANES, (j + 1) * LANES)
        value = conv(j * LANES, LANES)
        scaled = value * spread(steps, j * per)
        scaled_b = scaled.astype(jnp.bfloat16)
        inner = None
        for i in range(per):
            h = j * per + i
            gap = log_decay[:, h : h + 1] - log_decay_t[h : h + 1, :]
            score = cross * jnp.exp(jnp.where(causal, gap, -jnp.inf))
            part = dot32(score.astype(jnp.bfloat16), scaled_b)
            inner = part if inner is None else jnp.where(lane == i, part, inner)
        ld = spread(log_decay, j * per)
        last = ld[rows - 1 : rows, :]
        state = state_ref[0, :, cols]
        carried = dot32(read, state.astype(jnp.bfloat16)) * jnp.exp(ld)
        heads_ref[0, :, cols] = inner + carried + skip_ref[:, cols] * value
        faded = (scaled * jnp.exp(last - ld)).astype(jnp.bfloat16)
        state_ref[0, :, cols] = state * jnp.exp(last) + dot32(write_t, faded)


def gate_kernel(head_dim, heads_ref, read_ref, incoming_ref, reach_ref, gate_ref, gated_ref, square_ref):
    rows, channels = heads_ref.shape[1], heads_ref.shape[2]
    per = LANES // head_dim
    read = read_ref[0]
    reach = jnp.exp(reach_ref[0])
    lane = lax.broadcasted_iota(jnp.int32, (rows, LANES), 1) // head_dim
    squares = jnp.zeros((rows, LANES), jnp.float32)
    for j in range(channels // LANES):
        cols = slice(j * LANES, (j + 1) * LANES)
        scale = jnp.broadcast_to(reach[:, j * per : j * per + 1], (rows, LANES))
        for i in range(1, per):
            h = j * per + i
            scale = jnp.where(lane == i, jnp.broadcast_to(reach[:, h : h + 1], (rows, LANES)), scale)
        outer = dot32(read, incoming_ref[0, :, cols]) * scale
        gate = gate_ref[0, :, cols].astype(jnp.float32)
        gated = ((heads_ref[0, :, cols] + outer) * silu(gate)).astype(jnp.bfloat16)
        gated_ref[0, :, cols] = gated
        wide = gated.astype(jnp.float32)
        squares = squares + wide * wide
    square_ref[0] = jnp.broadcast_to(jnp.sum(squares, axis=1, keepdims=True), (rows, LANES))


def block_spec(rows, width):
    return pl.BlockSpec((1, rows, width), lambda s, b: (s, b, 0))


def seq_spec(rows, width):
    return pl.BlockSpec((1, rows, width), lambda s, b: (s, 0, 0))


def body(
    tokens,
    norm_gain,
    w_gate,
    w_value,
    w_write,
    w_read,
    w_step,
    conv_value,
    conv_write,
    conv_read,
    step_bias,
    decay_log,
    skip_gain,
    out_gain,
    w_out,
):
    seqs, own_rows, width = tokens.shape
    group = lax.axis_size("tp")
    rank = lax.axis_index("tp")
    local_heads = w_step.shape[1] // group
    channels = w_gate.shape[1]
    head_dim = channels // local_heads
    state_dim = w_write.shape[1]
    tap_count = conv_value.shape[0]
    rows = own_rows * group
    first_head = rank * local_heads

    def local(x, count, axis):
        return lax.dynamic_slice_in_dim(x, rank * count, count, axis)

    mix_part = jnp.concatenate([w_value, w_write, w_read], axis=1)
    w_mix = lax.all_gather(mix_part, "sp", axis=0, tiled=True)
    gate_part, w_mix = lax.optimization_barrier((w_gate, w_mix))
    whole_gate = lax.all_gather(gate_part, "sp", axis=0, tiled=True)
    out_part, whole_gate = lax.optimization_barrier((local(w_out, channels, 0), whole_gate))
    whole_out = lax.all_gather(out_part, "sp", axis=1, tiled=True)

    wide = tokens.astype(jnp.float32)
    scale = lax.rsqrt(jnp.mean(wide * wide, axis=-1, keepdims=True) + EPSILON)
    normed = (wide * scale * norm_gain).astype(jnp.bfloat16)
    flat = gather_tokens(normed, "tp").reshape(seqs * rows, width)

    step_raw = dot32(flat, local(w_step, local_heads, 1)).reshape(seqs, rows, local_heads)
    step_size = jax.nn.softplus(step_raw + local(step_bias, local_heads, 0))
    rate = -jnp.exp(local(decay_log, local_heads, 0))
    block = LANES if rows % LANES == 0 else rows
    blocks = rows // block
    lower = jnp.tril(jnp.ones((block, block), jnp.float32))
    change = (step_size * rate).reshape(seqs, blocks, block, local_heads)
    log_decay = jnp.einsum("lm,skmh->sklh", lower, change, precision=HIGHEST)
    log_decay_t = jnp.moveaxis(log_decay, 3, 1).reshape(seqs, local_heads, rows)
    block_total = log_decay[:, :, -1, :]
    run_sum = jnp.cumsum(block_total, axis=1)
    reach = ((run_sum - block_total)[:, :, None, :] + log_decay).reshape(seqs, rows, local_heads)
    log_decay = log_decay.reshape(seqs, rows, local_heads)
    dev_decay = jnp.repeat(jnp.exp(run_sum[:, -1:, :]), head_dim, axis=2)

    taps = jnp.concatenate(
        [local(conv_value, channels, 1), local(conv_write, state_dim, 1), local(conv_read, state_dim, 1)], axis=1
    )
    skip = jnp.repeat(local(skip_gain, local_heads, 0), head_dim)[None]

    mix = dot32(flat, w_mix).astype(jnp.bfloat16).reshape(seqs, rows, w_mix.shape[1])
    tail = shifted(mix[:, rows - tap_count + 1 :], "sp", 1)
    ext = jnp.concatenate([jnp.pad(tail, ((0, 0), (HALO - tap_count + 1, 0), (0, 0))), mix], axis=1)

    grid = (seqs, blocks)
    full = lambda a: pl.BlockSpec(a.shape, lambda s, b: (0,) * a.ndim)
    params = pltpu.CompilerParams(dimension_semantics=("arbitrary", "arbitrary"))
    heads, read_rows, state = pl.pallas_call(
        lambda *refs: mixer_kernel(head_dim, *refs),
        grid=grid,
        in_specs=[
            full(taps),
            full(skip),
            seq_spec(rows + HALO, ext.shape[2]),
            block_spec(block, local_heads),
            pl.BlockSpec((1, local_heads, block), lambda s, b: (s, 0, b)),
            block_spec(block, local_heads),
        ],
        out_specs=[block_spec(block, channels), block_spec(block, state_dim), seq_spec(state_dim, channels)],
        out_shape=[
            jax.ShapeDtypeStruct((seqs, rows, channels), jnp.float32),
            jax.ShapeDtypeStruct((seqs, rows, state_dim), jnp.bfloat16),
            jax.ShapeDtypeStruct((seqs, state_dim, channels), jnp.float32),
        ],
        compiler_params=params,
        cost_estimate=pl.CostEstimate(flops=20 * 10**9, bytes_accessed=8 * 2**20, transcendentals=0),
        name="mixer",
    )(taps, skip, ext, log_decay, log_decay_t, step_size)

    incoming = incoming_state(state, dev_decay, "sp").astype(jnp.bfloat16)

    gate_in = dot32(flat, whole_gate).astype(jnp.bfloat16).reshape(seqs, rows, channels)
    gated, squares = pl.pallas_call(
        lambda *refs: gate_kernel(head_dim, *refs),
        grid=grid,
        in_specs=[
            block_spec(block, channels),
            block_spec(block, state_dim),
            seq_spec(state_dim, channels),
            block_spec(block, local_heads),
            block_spec(block, channels),
        ],
        out_specs=[block_spec(block, channels), block_spec(block, LANES)],
        out_shape=[
            jax.ShapeDtypeStruct((seqs, rows, channels), jnp.bfloat16),
            jax.ShapeDtypeStruct((seqs, rows, LANES), jnp.float32),
        ],
        compiler_params=params,
        cost_estimate=pl.CostEstimate(flops=5 * 10**9, bytes_accessed=8 * 2**20, transcendentals=0),
        name="gating",
    )(heads, read_rows, incoming, reach, gate_in)

    square_sum = total_over(squares[:, :, :1], "tp")
    out_scale = lax.rsqrt(square_sum / (channels * group) + EPSILON)
    mixed_in = (gated.astype(jnp.float32) * out_scale * local(out_gain, channels, 0)).astype(jnp.bfloat16)

    if not is_power(group):
        partial = dot32(mixed_in.reshape(seqs * rows, channels), whole_out).reshape(seqs, rows, width)
        return lax.psum_scatter(partial, "tp", scatter_dimension=1, tiled=True).astype(jnp.bfloat16)

    bits = bits_of("tp")[::-1]
    pieces = mixed_in.reshape(seqs, group // 2, 2, own_rows, channels)

    def product(which):
        chosen = lax.dynamic_index_in_dim(pieces, which, 2, False)
        return dot32(chosen.reshape(-1, channels), whole_out).reshape(seqs, group // 2, own_rows, width)

    mine = rank & 1
    send = product(1 - mine).astype(jnp.bfloat16)
    got = swapped(send, "tp", 1)
    keep = product(mine) + got.astype(jnp.float32)
    for bit in bits[1:]:
        count = keep.shape[1]
        split = keep.reshape(seqs, count // 2, 2, own_rows, width)
        side = (rank // bit) & 1
        send = lax.dynamic_index_in_dim(split, 1 - side, 2, False).astype(jnp.bfloat16)
        kept = lax.dynamic_index_in_dim(split, side, 2, False)
        keep = kept + swapped(send, "tp", bit).astype(jnp.float32)
    return keep.reshape(seqs, own_rows, width).astype(jnp.bfloat16)


def solution(mesh):
    in_specs = (
        P(None, ("sp", "tp"), None),
        P(),
        P("sp", "tp"),
        P("sp", "tp"),
        P("sp", "tp"),
        P("sp", "tp"),
        P(),
        P(),
        P(),
        P(),
        P(),
        P(),
        P(),
        P(),
        P(None, "sp"),
    )
    out_specs = P(None, ("sp", "tp"), None)
    return jax.shard_map(body, mesh=mesh, in_specs=in_specs, out_specs=out_specs, check_vma=False)
```

time: 580 us -> 383 us (0.66)
  the two profiles are of different devices: /device:TPU:0 before, /device:TPU:16 now
where the time goes in v1:
time: 383 us; the launch traced here: 382 us
  waiting for transfers between devices  252 us (66%)
  matrix products  33.3 us (9%)
  other arithmetic  25.2 us (7%)
  starting transfers between devices  23.3 us (6%)
  Pallas kernels  22.9 us (6%)
  between operations  13.4 us (3%)
  local copies, waits for them, and re-layouts  11.9 us (3%)
    all_gather x1, waiting for transfers between devices, body(): w_mix = lax.all_gather(mix_part, 'sp', axis=0, tiled=True)  86.8 us
    ppermute x6, waiting for transfers between devices, shifted(): return lax.ppermute(x, axis, pairs)  67.8 us
    ppermute x6, waiting for transfers between devices, swapped(): return lax.ppermute(x, axis, [(i, i ^ bit) for i in range(devices)])  65.9 us
    dot_general x5, matrix products, dot32(): return jnp.dot(a, b, preferred_element_type=jnp.float32)  32.3 us
    all_gather x1, waiting for transfers between devices, body(): whole_gate = lax.all_gather(gate_part, 'sp', axis=0, tiled=True)  31.4 us
    ppermute x6, starting transfers between devices, shifted(): return lax.ppermute(x, axis, pairs)  18.5 us
    pallas_call x1, Pallas kernels, body(): pl.pallas_call(lambda *refs: mixer_kernel(head_dim, *refs), grid=grid, in...  14.7 us
    pallas_call x1, Pallas kernels, body(): pl.pallas_call(lambda *refs: gate_kernel(head_dim, *refs), grid=grid, in_...  8.28 us
  transfers between devices with their start and end apart: 15, of which 12 were waited for; matrix products, arithmetic and copies ran while one was open for 13% of the time, Pallas kernels for 6%

profile of v1, /device:TPU:16, one launch (start us, length us, event | category | flops | bytes accessed | tf_op | source)
XLA Modules:
  0.0 381.9 jit_solution(8500539202726743844)
XLA Ops:
  6.5 2.1 pad_maximum_fusion.1
  8.8 86.8 %all-gather.4.cloned.1.call-done = bf16[2048,1280]{1,0:T(8,128)(2,1)} async-done(((bf16[256,1280]{1,0:T(8,128)(2,1)}), bf16[2048,1280]{1,0:T(8,128)(2,1)}) %all-gather.4.cloned.1.call-update) | async-done | bytes 5242896 | tf_op jit(solution)/shard_map/all_gather | solution.py:219
  96.0 1.3 fusion.18
  97.3 1.5 collective-permute-start
  98.7 22.7 %collective-permute-done = bf16[2,1,128,2048]{3,2,0,1:T(8,128)(2,1)} collective-permute-done((bf16[2,1,128,2048]{3,2,0,1:T(8,128)(2,1)}, bf16[2,1,128,2048]{3,2,0,1:T(8,128)(2,1)}, u32[]{:S(2)}, u32[]{:S(2)}) %collective-permute-start) | collective-permute-done | bytes 1048608 | tf_op jit(solution)/shard_map/ppermute | solution.py:22
  121.5 1.9 select_bitcast_fusion.3
  123.5 0.9 copy-done.3
  124.4 1.6 maximum_bitcast_fusion
  127.7 0.7 constant_dynamic-slice_fusion.3
  128.4 0.8 constant_dynamic-slice_fusion
  130.5 2.8 select_bitcast_fusion.1
  133.7 3.1 broadcast_multiply_fusion
  136.8 1.0 fusion.28
  137.7 31.4 %all-gather.6.cloned.1.call-done = bf16[2048,1024]{1,0:T(8,128)(2,1)} async-done(((bf16[256,1024]{1,0:T(8,128)(2,1)}), bf16[2048,1024]{1,0:T(8,128)(2,1)}) %all-gather.6.cloned.1.call-update) | async-done | bytes 4194320 | tf_op jit(solution)/shard_map/all_gather | solution.py:221
  169.2 8.9 %convolution_convert_fusion = bf16[1024,1280]{1,0:T(8,128)(2,1)S(1)} fusion(bf16[1024,2048]{1,0:T(8,128)(2,1)} %bitcast.83, bf16[2048,1280]{1,0:T(8,128)(2,1)} %all-gather.4.cloned.1.call-done), kind=kOutput, calls=%fused_computation.9 | convolution fusion | flops 5370019840 | bytes 12058624 | tf_op jit(solution)/shard_map/dot_general | solution.py:91
  178.1 1.5 copy-done.7
  179.6 2.5 collective-permute-start.2
  182.7 1.0 copy.36
  183.7 3.0 collective-permute-done.2
  186.7 3.4 fusion.8.refs_2_
  190.2 14.7 %mixer.1 = (f32[2,512,1024]{2,1,0:T(8,128)}, bf16[2,512,128]{2,1,0:T(8,128)(2,1)}, f32[2,128,1024]{2,1,0:T(8,128)}) custom-call(f32[4,1280]{1,0:T(4,128)} %pad_maximum_fusion.2.refs_0_, f32[1,1024]{1,0:T(1,128)} %broadcast_in_dim_reshape.3.refs_1_, bf16[2,528,1280]{2,1,0:T(8,128)(2,1)} %fusion.8.refs_2_, f32[2,512,16]{2,1,0:T(8,128)} %bitcast.94, ...), custom_call_target="tpu_custom_call" | custom-call | flops 20000000000 | bytes 8388608 | tf_op jit(solution)/shard_map/mixer/pallas_call | solution.py:257
  204.8 1.4 convert_element_type.64
  206.3 1.9 collective-permute-start.3
  208.6 29.3 %collective-permute-done.3 = bf16[2,128,1024]{2,1,0:T(8,128)(2,1)S(1)} collective-permute-done((bf16[2,128,1024]{2,1,0:T(8,128)(2,1)S(1)}, bf16[2,128,1024]{2,1,0:T(8,128)(2,1)S(1)}, u32[]{:S(2)}, u32[]{:S(2)}) %collective-permute-start.3) | collective-permute-done | bytes 524320 | tf_op jit(solution)/shard_map/ppermute | solution.py:17
  237.9 1.4 fusion.27
  239.3 6.6 %collective-permute-start.4 = (bf16[2,128,1024]{2,1,0:T(8,128)(2,1)S(1)}, bf16[2,128,1024]{2,1,0:T(8,128)(2,1)S(1)}, u32[]{:S(2)}, u32[]{:S(2)}) collective-permute-start(bf16[2,128,1024]{2,1,0:T(8,128)(2,1)S(1)} %fusion.27), channel_id=1, source_target_pairs={{0,8},{4,12},{8,16},{12,20},{16,24},{20,28},{1,9},{5,13},{9,17},{1... | collective-permute-start | bytes 1572872 | tf_op jit(solution)/shard_map/ppermute | solution.py:17
  246.0 1.9 collective-permute-start.5
  248.0 15.7 %collective-permute-done.5 = f32[2,1,1024]{2,0,1:T(2,128)S(1)} collective-permute-done((f32[2,1,1024]{2,0,1:T(2,128)S(1)}, f32[2,1,1024]{2,0,1:T(2,128)S(1)}, u32[]{:S(2)}, u32[]{:S(2)}) %collective-permute-start.5) | collective-permute-done | bytes 8224 | tf_op jit(solution)/shard_map/ppermute | solution.py:17
  264.0 1.3 collective-permute-start.6
  265.5 4.3 %collective-permute-start.7 = (f32[2,1,1024]{2,0,1:T(2,128)S(1)}, f32[2,1,1024]{2,0,1:T(2,128)S(1)}, u32[]{:S(2)}, u32[]{:S(2)}) collective-permute-start(f32[2,1,1024]{2,0,1:T(2,128)S(1)} %mul.116), channel_id=1, source_target_pairs={{0,8},{4,12},{8,16},{12,20},{16,24},{20,28},{1,9},{5,13},{9,17},{1... | collective-permute-start | bytes 24584 | tf_op jit(solution)/shard_map/ppermute | solution.py:17
  269.9 1.0 copy.39
  270.9 19.7 %collective-permute-done.7 = f32[2,1,1024]{2,0,1:T(2,128)S(1)} collective-permute-done((f32[2,1,1024]{2,0,1:T(2,128)S(1)}, f32[2,1,1024]{2,0,1:T(2,128)S(1)}, u32[]{:S(2)}, u32[]{:S(2)}) %collective-permute-start.7) | collective-permute-done | bytes 8224 | tf_op jit(solution)/shard_map/ppermute | solution.py:17
  290.6 1.1 fusion.14.refs_2_
  291.7 9.3 %convolution_convert_fusion.1 = bf16[1024,1024]{1,0:T(8,128)(2,1)} fusion(bf16[1024,2048]{1,0:T(8,128)(2,1)} %bitcast.84, bf16[2048,1024]{1,0:T(8,128)(2,1)} %all-gather.6.cloned.1.call-done), kind=kOutput, calls=%fused_computation.22 | convolution fusion | flops 4296015872 | bytes 10485760 | tf_op jit(solution)/shard_map/dot_general | solution.py:91
  301.0 8.3 %gating.1 = (bf16[2,512,1024]{2,1,0:T(8,128)(2,1)}, f32[2,512,128]{2,1,0:T(8,128)}) custom-call(f32[2,512,1024]{2,1,0:T(8,128)} %get-tuple-element.15.refs_0_, bf16[2,512,128]{2,1,0:T(8,128)(2,1)} %get-tuple-element.16.refs_1_, bf16[2,128,1024]{2,1,0:T(8,128)(2,1)} %fusion.14.refs_2_, f32[2,512,16]{2,1,0:T(8,128)} %bitcast.93, bf16[2,512,1024]{2,1,0:T(8,128)(2,1)} %bitcast.100), custom_call_target="tpu_custom_call" | custom-call | flops 5000000000 | bytes 8388608 | tf_op jit(solution)/shard_map/gating/pallas_call | solution.py:282
  309.2 1.5 collective-permute-start.8
  310.8 12.3 %collective-permute-done.8 = f32[2,512,1]{2,1,0:T(8,128)S(1)} collective-permute-done((f32[2,512,1]{2,1,0:T(8,128)}, f32[2,512,1]{2,1,0:T(8,128)S(1)}, u32[]{:S(2)}, u32[]{:S(2)}) %collective-permute-start.8) | collective-permute-done | bytes 4128 | tf_op jit(solution)/shard_map/ppermute | solution.py:22
  323.1 1.1 slice_add_fusion
  324.2 1.9 collective-permute-done.9
  326.4 2.1 multiply_convert_fusion
  328.5 5.8 %fusion.5 = bf16[2,2,128,2048]{3,2,1,0:T(8,128)(2,1)} fusion(bf16[1024,2048]{1,0:T(8,128)(2,1)} %all-gather.8.cloned.1.call-done, bf16[2,2,2,128,1024]{4,3,2,1,0:T(8,128)(2,1)S(1)} %bitcast.90, s32[]{:T(128)S(6)} %select_n.78), kind=kOutput, calls=%fused_computation.10 | convolution fusion | flops 2148532224 | bytes 7340036 | tf_op jit(solution)/shard_map/dot_general | solution.py:91
  334.5 4.4 %collective-permute-done.10 = bf16[2,2,128,2048]{3,2,1,0:T(8,128)(2,1)} collective-permute-done((bf16[2,2,128,2048]{3,2,1,0:T(8,128)(2,1)}, bf16[2,2,128,2048]{3,2,1,0:T(8,128)(2,1)}, u32[]{:S(2)}, u32[]{:S(2)}) %collective-permute-start.10) | collective-permute-done | bytes 2097184 | tf_op jit(solution)/shard_map/ppermute | solution.py:22
  338.9 5.2 %convert_add_fusion = f32[2,2,128,2048]{3,2,1,0:T(8,128)S(1)} fusion(bf16[2,2,128,2048]{3,2,1,0:T(8,128)(2,1)} %collective-permute-done.10, bf16[1024,2048]{1,0:T(8,128)(2,1)} %all-gather.8.cloned.1.call-done, bf16[2,2,2,128,1024]{4,3,2,1,0:T(8,128)(2,1)S(1)} %bitcast.91, s32[]{:T(128)S(6)} %select_n.77), kind=kOutput, calls=%fused_computation.7 | convolution fusion | flops 2149580800 | bytes 11534340 | tf_op jit(solution)/shard_map/dot_general | solution.py:91
  344.1 1.9 copy-done.8
  346.0 1.1 dynamic-slice_convert_fusion
  347.1 1.5 collective-permute-start.11
  348.6 24.0 %collective-permute-done.11 = bf16[2,1,128,2048]{3,2,1,0:T(8,128)(2,1)S(1)} collective-permute-done((bf16[2,1,128,2048]{3,2,1,0:T(8,128)(2,1)}, bf16[2,1,128,2048]{3,2,1,0:T(8,128)(2,1)S(1)}, u32[]{:S(2)}, u32[]{:S(2)}) %collective-permute-start.11) | collective-permute-done | bytes 1048608 | tf_op jit(solution)/shard_map/ppermute | solution.py:22
  372.6 2.9 fusion.17
  (63 shorter events, 6.0 us)
Async XLA Ops:
  6.5 121.9 %copy-start = (bf16[4096,256]{1,0:T(8,128)(2,1)S(1)}, bf16[4096,256]{1,0:T(8,128)(2,1)}, u32[]{:S(2)}) copy-start(bf16[4096,256]{1,0:T(8,128)(2,1)} %param.29) | copy-start | bytes 6291460
  6.5 89.1 %copy-start.2 = (bf16[2,128,2048]{2,1,0:T(8,128)(2,1)S(1)}, bf16[2,128,2048]{2,1,0:T(8,128)(2,1)}, u32[]{:S(2)}) copy-start(bf16[2,128,2048]{2,1,0:T(8,128)(2,1)} %param.15) | copy-start | bytes 3145732
  6.5 89.5 %copy-start.9 = (f32[2048]{0:T(1024)S(1)}, f32[2048]{0:T(1024)}, u32[]{:S(2)}) copy-start(f32[2048]{0:T(1024)} %param.16) | copy-start | bytes 24580
  6.5 89.1 %all-gather.4.cloned.1.call-start = ((), (), s32[]{:S(2)}) async-start(), calls=%async_computation | async-start | bytes 5898240 | tf_op jit(solution)/shard_map/all_gather | solution.py:219
  8.7 160.4 %all-gather.6.cloned.1.call-start = ((), (), s32[]{:S(2)}) async-start(), calls=%async_computation.1 | async-start | bytes 4718592 | tf_op jit(solution)/shard_map/all_gather | solution.py:221
  95.6 232.9 %all-gather.8.cloned.1.call-start = ((), (), s32[]{:S(2)}) async-start(), calls=%async_computation.2 | async-start | bytes 4718592 | tf_op jit(solution)/shard_map/all_gather | solution.py:223
  97.3 24.2 %collective-permute-start = (bf16[2,1,128,2048]{3,2,0,1:T(8,128)(2,1)}, bf16[2,1,128,2048]{3,2,0,1:T(8,128)(2,1)}, u32[]{:S(2)}, u32[]{:S(2)}) collective-permute-start(bf16[2,1,128,2048]{3,2,0,1:T(8,128)(2,1)} %fusion.18), channel_id=1, source_target_pairs={{0,2},{1,3},{2,0},{3,1},{4,6},{5,7},{6,4},{7,5},{8,10},{9,11},{10,... | collective-permute-start | bytes 3145736 | tf_op jit(solution)/shard_map/ppermute | solution.py:22
  123.4 1.0 copy-start.3
  123.4 2.6 copy-start.4
  123.4 2.6 copy-start.10
  123.4 2.6 copy-start.11
  123.4 3.4 copy-start.12
  126.0 4.5 %collective-permute-start.1 = (bf16[2,2,128,2048]{3,2,1,0:T(8,128)(2,1)}, bf16[2,2,128,2048]{3,2,1,0:T(8,128)(2,1)}, u32[]{:S(2)}, u32[]{:S(2)}) collective-permute-start(bf16[2,2,128,2048]{3,2,1,0:T(8,128)(2,1)} %maximum_bitcast_fusion), channel_id=1, source_target_pairs={{0,1},{1,0},{2,3},{3,2},{4,5},{5,4},{6,7},{7,6},{8,9},{9,8},{10,11... | collective-permute-start | bytes 6291464 | tf_op jit(solution)/shard_map/ppermute | solution.py:22
  133.7 3.1 copy-start.6
  178.1 1.5 copy-start.7
  179.6 7.1 %collective-permute-start.2 = (bf16[2,3,1280]{2,1,0:T(4,128)(2,1)S(1)}, bf16[2,3,1280]{2,1,0:T(4,128)(2,1)S(1)}, u32[]{:S(2)}, u32[]{:S(2)}) collective-permute-start(bf16[2,3,1280]{2,1,0:T(4,128)(2,1)S(1)} %slice.16), channel_id=1, source_target_pairs={{0,4},{4,8},{8,12},{12,16},{16,20},{20,24},{24,28},{1,5},{5,9},{9,... | collective-permute-start | bytes 46088 | tf_op jit(solution)/shard_map/ppermute | solution.py:17
  204.8 58.9 %copy-start.5 = (f32[2,128,1024]{2,1,0:T(8,128)S(1)}, f32[2,128,1024]{2,1,0:T(8,128)}, u32[]{:S(2)}) copy-start(f32[2,128,1024]{2,1,0:T(8,128)} %get-tuple-element.17) | copy-start | bytes 3145732
  206.3 31.7 %collective-permute-start.3 = (bf16[2,128,1024]{2,1,0:T(8,128)(2,1)S(1)}, bf16[2,128,1024]{2,1,0:T(8,128)(2,1)S(1)}, u32[]{:S(2)}, u32[]{:S(2)}) collective-permute-start(bf16[2,128,1024]{2,1,0:T(8,128)(2,1)S(1)} %convert_element_type.64), channel_id=1, source_target_pairs={{0,4},{4,8},{8,12},{12,16},{16,20},{20,24},{24,28},{1,5},{5,9},{9,... | collective-permute-start | bytes 1572872 | tf_op jit(solution)/shard_map/ppermute | solution.py:17
  239.3 24.4 %collective-permute-start.4 = (bf16[2,128,1024]{2,1,0:T(8,128)(2,1)S(1)}, bf16[2,128,1024]{2,1,0:T(8,128)(2,1)S(1)}, u32[]{:S(2)}, u32[]{:S(2)}) collective-permute-start(bf16[2,128,1024]{2,1,0:T(8,128)(2,1)S(1)} %fusion.27), channel_id=1, source_target_pairs={{0,8},{4,12},{8,16},{12,20},{16,24},{20,28},{1,9},{5,13},{9,17},{1... | collective-permute-start | bytes 1572872 | tf_op jit(solution)/shard_map/ppermute | solution.py:17
  246.0 17.7 %collective-permute-start.5 = (f32[2,1,1024]{2,0,1:T(2,128)S(1)}, f32[2,1,1024]{2,0,1:T(2,128)S(1)}, u32[]{:S(2)}, u32[]{:S(2)}) collective-permute-start(f32[2,1,1024]{2,0,1:T(2,128)S(1)} %broadcast_in_dim.28), channel_id=1, source_target_pairs={{0,4},{4,8},{8,12},{12,16},{16,20},{20,24},{24,28},{1,5},{5,9},{9,... | collective-permute-start | bytes 24584 | tf_op jit(solution)/shard_map/ppermute | solution.py:17
  264.0 26.6 %collective-permute-start.6 = (bf16[2,128,1024]{2,1,0:T(8,128)(2,1)S(1)}, bf16[2,128,1024]{2,1,0:T(8,128)(2,1)S(1)}, u32[]{:S(2)}, u32[]{:S(2)}) collective-permute-start(bf16[2,128,1024]{2,1,0:T(8,128)(2,1)S(1)} %fusion.16), channel_id=1, source_target_pairs={{0,16},{4,20},{8,24},{12,28},{1,17},{5,21},{9,25},{13,29},{2,18},{... | collective-permute-start | bytes 1572872 | tf_op jit(solution)/shard_map/ppermute | solution.py:17
  265.5 25.1 %collective-permute-start.7 = (f32[2,1,1024]{2,0,1:T(2,128)S(1)}, f32[2,1,1024]{2,0,1:T(2,128)S(1)}, u32[]{:S(2)}, u32[]{:S(2)}) collective-permute-start(f32[2,1,1024]{2,0,1:T(2,128)S(1)} %mul.116), channel_id=1, source_target_pairs={{0,8},{4,12},{8,16},{12,20},{16,24},{20,28},{1,9},{5,13},{9,17},{1... | collective-permute-start | bytes 24584 | tf_op jit(solution)/shard_map/ppermute | solution.py:17
  309.2 17.1 %dynamic-slice-start = ((f32[4096]{0:T(1024)}, s32[]{:T(128)}), f32[1024]{0:T(1024)S(1)}, s32[]{:S(2)}) async-start(f32[4096]{0:T(1024)} %param.28, s32[]{:T(128)} %select_n.66), calls=%async_computation.3 | async-start | bytes 8704 | tf_op jit(solution)/shard_map/dynamic_slice | solution.py:216
  309.2 13.8 %collective-permute-start.8 = (f32[2,512,1]{2,1,0:T(8,128)}, f32[2,512,1]{2,1,0:T(8,128)S(1)}, u32[]{:S(2)}, u32[]{:S(2)}) collective-permute-start(f32[2,512,1]{2,1,0:T(8,128)} %bitcast.92), channel_id=1, source_target_pairs={{0,2},{1,3},{2,0},{3,1},{4,6},{5,7},{6,4},{7,5},{8,10},{9,11},{10,... | collective-permute-start | bytes 12296 | tf_op jit(solution)/shard_map/ppermute | solution.py:22
  324.2 2.0 collective-permute-start.9
  334.4 4.5 %collective-permute-start.10 = (bf16[2,2,128,2048]{3,2,1,0:T(8,128)(2,1)}, bf16[2,2,128,2048]{3,2,1,0:T(8,128)(2,1)}, u32[]{:S(2)}, u32[]{:S(2)}) collective-permute-start(bf16[2,2,128,2048]{3,2,1,0:T(8,128)(2,1)} %fusion.5), channel_id=1, source_target_pairs={{0,1},{1,0},{2,3},{3,2},{4,5},{5,4},{6,7},{7,6},{8,9},{9,8},{10,11... | collective-permute-start | bytes 6291464 | tf_op jit(solution)/shard_map/ppermute | solution.py:22
  344.1 2.0 copy-start.8
  346.0 29.4 %copy-start.1 = (bf16[4096,256]{1,0:T(8,128)(2,1)S(1)}, bf16[4096,256]{1,0:T(8,128)(2,1)}, u32[]{:S(2)}) copy-start(bf16[4096,256]{1,0:T(8,128)(2,1)} %param.29) | copy-start | bytes 6291460
  347.1 25.4 %collective-permute-start.11 = (bf16[2,1,128,2048]{3,2,1,0:T(8,128)(2,1)}, bf16[2,1,128,2048]{3,2,1,0:T(8,128)(2,1)S(1)}, u32[]{:S(2)}, u32[]{:S(2)}) collective-permute-start(bf16[2,1,128,2048]{3,2,1,0:T(8,128)(2,1)} %dynamic-slice_convert_fusion), channel_id=1, source_target_pairs={{0,2},{1,3},{2,0},{3,1},{4,6},{5,7},{6,4},{7,5},{8,10},{9,11},{10,... | collective-permute-start | bytes 3145736 | tf_op jit(solution)/shard_map/ppermute | solution.py:22
Sparse Core Ops, SparseCore 0:
  9.5 86.0 all-gather.3
  97.7 71.3 all-gather.5
  171.2 86.7 all-gather.7
